TPU v7x, 512 devices: a whole 4x8x8 slice. The times are simulated.
512 devices in a mesh: ep: 32 (over z, x), tp: 16 (over y, core).
Axes of the slice: x: 4, y: 8, z: 8, core: 2. Of those that a mesh axis runs over, the one named last changes fastest.
Arguments:
- tokens_a: bfloat16 [4096, 2048], P('ep'), may hold values from -6 to 6
- gain_a: float32 [2048], replicated, may hold values from 0.1 to 1.9
- value_w: bfloat16 [2048, 2048], P(None, 'tp'), may hold values from -0.125 to 0.125
- gate_w: bfloat16 [2048, 2048], P(None, 'tp'), may hold values from -0.125 to 0.125
- kernel: float32 [31, 2048], P(None, 'tp')
- chan_gain: float32 [2048], P('tp'), may hold values from 0.1 to 1.9
- out_w: bfloat16 [2048, 2048], P('tp'), may hold values from -0.125 to 0.125
- tokens_b: bfloat16 [6144, 2048], P('ep'), may hold values from -6 to 6
- gain_b: float32 [2048], replicated, may hold values from 0.1 to 1.9
- routes: int32 [6144, 2], P('ep'), may hold values from 0 to 31, all different within a row; in each aligned block of 192 rows (0 to 191, 192 to 383, ...) at most 18 rows name the same one
- route_logits: float32 [6144, 2], P('ep'), may hold values from -6 to 6
- expert_gate: bfloat16 [32, 2048, 2816], P('ep', None, 'tp'), may hold values from -0.125 to 0.125
- expert_up: bfloat16 [32, 2048, 2816], P('ep', None, 'tp'), may hold values from -0.125 to 0.125
- expert_down: bfloat16 [32, 2816, 2048], P('ep', 'tp'), may hold values from -0.109375 to 0.109375
Outputs:
- conv_out: bfloat16 [2048, 4096], P('tp', 'ep')
- moe_out: bfloat16 [2048, 6144], P('tp', 'ep')
Inputs may be any that keep to these rules, and one draw needn't show every extreme that they name: `routes`: each row names 2 different experts; among the rows of one index of ep no expert is named by more than 18 rows, a bound that some block reaches.
All inputs are finite; a program needn't handle non-finite values.
Results may differ from a plain program's by a relative error of at most 0.018.
Values may be sent and summed in bfloat16 or wider, within the bound.
A program may use at most 64 MiB of HBM per device.

v0:
```python
import jax
import jax.numpy as jnp
from jax import lax
from jax.sharding import Mesh
from jax.sharding import PartitionSpec as P

CONV_CH = 2048
TP = ("tp_0", "tp_1")


def from_behind(block, axis, distance):
    devices = range(lax.axis_size(axis))
    route = [(i - distance, i) for i in devices if i - distance in devices]
    return lax.ppermute(block, axis, route)


def copy_for_each(x, axis):
    peers = lax.axis_size(axis)
    return lax.all_to_all(jnp.broadcast_to(x[None], (peers, *x.shape)), axis, 0, 0, tiled=True)


def taken_together(x, axis):
    return copy_for_each(x, axis).sum(axis=0)


def in_one(arrays, axis):
    ends = [0]
    for a in arrays:
        ends.append(ends[-1] + a.size)
    so_far = taken_together(jnp.concatenate([a.ravel() for a in arrays]), axis)
    return tuple((so_far[b:e].reshape(a.shape) for a, b, e in zip(arrays, ends, ends[1:])))


def in_blocks(x, dim, peers):
    before, after = (x.shape[:dim], x.shape[dim + 1 :])
    return jnp.moveaxis(x.reshape(*before, peers, -1, *after), dim, 0)


def sum_at_owner(x, axis, dim):
    peers = lax.axis_size(axis)
    tiles = lax.all_to_all(in_blocks(x, dim, peers), axis, 0, 0, tiled=True)
    return jnp.sum(tiles.astype(jnp.float32), axis=0)


def summed_rows(terms, axes):
    so_far = terms.astype(jnp.bfloat16)
    for axis in axes:
        so_far = lax.psum_scatter(so_far, axis, scatter_dimension=0, tiled=True)
    return so_far.astype(jnp.float32)


def rms_scaled(tokens, gain):
    values = tokens.astype(jnp.float32)
    scaled = values * lax.rsqrt(jnp.mean(values * values, axis=1, keepdims=True) + 1e-06)
    return (scaled * gain[None, :]).astype(jnp.bfloat16)


def slot_table(route_rows, experts, capacity):
    flat_expert = route_rows.reshape(-1)
    expert_ids = jnp.arange(experts, dtype=jnp.int32)
    onehot = (flat_expert[:, None] == expert_ids[None, :]).astype(jnp.int32)
    before = jnp.cumsum(onehot, axis=0) - onehot
    ranking = jnp.sum(before * onehot, axis=1)
    return flat_expert * capacity + ranking


def body(
    tokens_a,
    gain_a,
    value_w,
    gate_w,
    kernel,
    chan_gain,
    out_w,
    tokens_b,
    gain_b,
    routes,
    route_logits,
    expert_gate,
    expert_up,
    expert_down,
):
    normed = rms_scaled(tokens_a, gain_a)
    contract_first = (((0,), (1,)), ((), ()))
    value_part = lax.dot_general(
        value_w, normed, contract_first, preferred_element_type=jnp.float32
    )
    gate_part = lax.dot_general(gate_w, normed, contract_first, preferred_element_type=jnp.float32)
    glu = (value_part * jax.nn.sigmoid(gate_part)).astype(jnp.bfloat16)
    taps = kernel.shape[0]
    length = glu.shape[1]
    rim = from_behind(glu[:, length - (taps - 1) :], "ep", 1)
    padded = jnp.concatenate([rim, glu], axis=1).astype(jnp.float32)
    mixed = jnp.zeros(glu.shape, jnp.float32)
    for tap in range(taps):
        mixed = mixed + kernel[tap][:, None] * padded[:, tap : tap + length]
    chan_total, chan_square = in_one((jnp.sum(mixed, axis=0), jnp.sum(mixed * mixed, axis=0)), TP)
    average = chan_total / CONV_CH
    spread = chan_square / CONV_CH - average * average
    normal_out = (
        (mixed - average[None, :]) * lax.rsqrt(spread + 1e-05)[None, :] * chan_gain[:, None]
    )
    activated = jax.nn.silu(normal_out).astype(jnp.bfloat16)
    block_w = out_w
    conv_out = sum_at_owner(
        lax.dot_general(
            block_w, activated, (((0,), (0,)), ((), ())), preferred_element_type=jnp.float32
        ).astype(jnp.bfloat16),
        TP,
        0,
    ).astype(jnp.bfloat16)
    normed_b = rms_scaled(tokens_b, gain_b)
    experts = lax.axis_size("ep")
    token_count = tokens_b.shape[0]
    choices_per = routes.shape[1]
    capacity = 3 * token_count * choices_per // (2 * experts)
    slots = slot_table(routes, experts, capacity)
    owner = jnp.arange(slots.shape[0], dtype=jnp.int32) // choices_per
    filled = jnp.zeros((experts * capacity,), jnp.int32).at[slots].set(owner + 1)
    own = lax.axis_index(TP)
    width = normed_b.shape[1] // lax.axis_size(TP)
    part = lax.dynamic_slice_in_dim(normed_b, own * width, width, axis=1)
    picked = jnp.take(part, jnp.maximum(filled - 1, 0), axis=0)
    send_rows = jnp.where((filled > 0)[:, None], picked, jnp.zeros_like(picked)).reshape(
        experts, capacity, -1
    )
    weights = jax.nn.softmax(route_logits, axis=1).reshape(-1)
    slot_ids = jnp.arange(experts * capacity, dtype=jnp.int32)
    combine = (
        ((slots[:, None] == slot_ids[None, :]).astype(jnp.float32) * weights[:, None])
        .reshape(token_count, choices_per, -1)
        .sum(axis=1)
    )
    gate_local = expert_gate[0]
    up_local = expert_up[0]
    arrived = lax.all_to_all(send_rows, "ep", split_axis=0, concat_axis=0, tiled=True).reshape(
        experts * capacity, -1
    )
    arrived = lax.all_gather(arrived, TP, axis=1, tiled=True)
    gate_act = jnp.dot(arrived, gate_local, preferred_element_type=jnp.float32)
    up_act = jnp.dot(arrived, up_local, preferred_element_type=jnp.float32)
    hidden = (jax.nn.silu(gate_act) * up_act).astype(jnp.bfloat16)
    down_local = expert_down[0]
    block_w = down_local
    expert_rows = summed_rows(
        lax.dot_general(
            block_w, hidden, (((0,), (1,)), ((), ())), preferred_element_type=jnp.float32
        ),
        TP,
    ).astype(jnp.bfloat16)
    returned = lax.all_to_all(
        expert_rows.reshape(expert_rows.shape[0], experts, capacity),
        "ep",
        split_axis=1,
        concat_axis=1,
        tiled=True,
    )
    returned_flat = returned.reshape(returned.shape[0], -1).astype(jnp.float32)
    moe_out = lax.dot_general(
        returned_flat,
        combine,
        (((1,), (1,)), ((), ())),
        precision=lax.Precision.HIGHEST,
        preferred_element_type=jnp.float32,
    )
    return (conv_out, moe_out.astype(jnp.bfloat16))


def solution(mesh):
    finer = Mesh(mesh.devices.reshape(mesh.shape["ep"], 8, 2), ("ep", "tp_0", "tp_1"))
    return jax.shard_map(
        body,
        mesh=finer,
        in_specs=(
            P("ep", None),
            P(),
            P(None, TP),
            P(None, TP),
            P(None, TP),
            P(TP),
            P(TP, None),
            P("ep", None),
            P(),
            P("ep", None),
            P("ep", None),
            P("ep", None, TP),
            P("ep", None, TP),
            P("ep", TP, None),
        ),
        out_specs=(P(TP, "ep"), P(TP, "ep")),
        check_vma=False,
    )
```

profile of v0, /device:TPU:8, one launch (start us, length us, event | category | flops | bytes accessed | tf_op | source)
XLA Modules:
  0.0 196.1 jit_solution(15484870692354183152)
XLA Ops:
  7.3 1.4 convert_element_type.61
  8.7 0.2 multiply_reduce_fusion
  8.9 0.1 copy.52
  9.0 0.1 eq.43
  9.2 0.1 eq.39
  9.3 0.9 reduce-window.6
  10.2 0.2 slice_reduce_fusion
  10.5 0.1 fusion.58
  10.6 0.1 reduce_sum.96
  10.8 0.1 mul.528
  10.9 2.9 %scatter_custom_fusion = s32[576]{0:T(1024)S(1)} fusion(s32[384]{0:T(512)S(1)} %fusion.70, s32[384]{0:T(512)S(1)} %fusion.64, s32[]{:T(128)} %constant.74.clone.1), kind=kCustom, calls=%fused_computation.130 | custom fusion | bytes 2308 | tf_op jit(solution)/shard_map/scatter | solution.py:119
  13.9 0.8 dynamic-slice
  14.7 0.1 fusion.25
  14.8 1.9 gather_fusion
  16.8 0.1 broadcast_in_dim.29
  16.9 0.1 broadcast_in_dim.50
  17.0 0.3 select_select_fusion
  17.3 24.6 %all_to_all.21 = bf16[32,18,128]{2,1,0:T(8,128)(2,1)S(1)} all-to-all(bf16[32,18,128]{2,1,0:T(8,128)(2,1)S(1)} %select_select_fusion), channel_id=1, replica_groups=mesh['ep'=32,'tp_0'=8,'tp_1'=2] {'ep'}, dimensions={0} | all-to-all | bytes 294912 | tf_op jit(solution)/shard_map/all_to_all | solution.py:136
  41.9 0.7 reshape.162
  42.7 0.0 reduce-scatter.5.cloned.1.call-start
  42.7 39.2 %all-gather.2.cloned.1.call-done = bf16[576,2048]{1,0:T(8,128)(2,1)} async-done(((bf16[576,128]{1,0:T(8,128)(2,1)}), bf16[576,2048]{1,0:T(8,128)(2,1)}) %all-gather.2.cloned.1.call-update) | async-done | bytes 2359312 | tf_op jit(solution)/shard_map/all_gather | solution.py:139
  81.9 3.8 %fusion.14 = f32[576,176]{0,1:T(8,128)} fusion(bf16[576,2048]{1,0:T(8,128)(2,1)} %all-gather.2.cloned.1.call-done, bf16[1,2048,176]{1,2,0:T(8,128)(2,1)} %param.25), kind=kOutput, calls=%fused_computation.26 | convolution fusion | flops 415236096 | bytes 3485696 | tf_op jit(solution)/shard_map/dot_general | solution.py:140
  85.7 4.7 %fusion = bf16[2048,576]{0,1:T(8,128)(2,1)} fusion(bf16[576,2048]{1,0:T(8,128)(2,1)S(1)} %copy-done.8, bf16[1,176,2048]{2,1,0:T(8,128)(2,1)S(1)} %copy-done, bf16[1,2048,176]{1,2,0:T(8,128)(2,1)} %param.26, f32[576,176]{0,1:T(8,128)} %fusion.14), kind=kOutput, calls=%fused_computation.3 | convolution fusion | flops 832260096 | bytes 6565888 | tf_op jit(solution)/shard_map/dot_general | solution.py:146
  90.4 1.0 copy-done.3
  91.5 0.2 fusion.8
  91.7 0.4 fusion.5
  92.1 0.1 copy.48
  92.2 0.4 fusion.7
  92.6 3.4 %collective-permute-start = (bf16[128,30]{0,1:T(8,128)(2,1)S(1)}, bf16[128,30]{0,1:T(8,128)(2,1)S(1)}, u32[]{:S(2)}, u32[]{:S(2)}) collective-permute-start(bf16[128,30]{0,1:T(8,128)(2,1)S(1)} %slice.270), channel_id=1, source_target_pairs={{0,16},{16,32},{32,48},{48,64},{64,80},{80,96},{96,112},{112,128},... | collective-permute-start | bytes 23048 | tf_op jit(solution)/shard_map/ppermute | solution.py:14
  96.0 1.3 collective-permute-done
  97.3 0.3 fusion.76
  97.7 11.6 %all_to_all.22 = f32[16,1,256]{2,1,0:T(1,128)S(1)} all-to-all(f32[16,1,256]{2,1,0:T(1,128)S(1)} %broadcast_in_dim.28), channel_id=1, replica_groups=mesh['ep'=32,'tp_0'=8,'tp_1'=2] {'tp_0','tp_1'}, dimensions={0} | all-to-all | bytes 32768 | tf_op jit(solution)/shard_map/all_to_all | solution.py:19
  109.3 0.4 fusion.1
  109.7 0.9 copy.69
  110.6 4.8 %all-to-all-start.1 = ((bf16[16,128,128]{1,2,0:T(8,128)(2,1)}), bf16[16,128,128]{1,2,0:T(8,128)(2,1)S(1)}, u32[]{:S(2)}, u32[]{:S(2)}) async-start(bf16[16,128,128]{1,2,0:T(8,128)(2,1)} %bitcast.112), calls=%async_computation.1 | async-start | bytes 1048576 | tf_op jit(solution)/shard_map/all_to_all | solution.py:41
  115.5 29.8 %reduce-scatter.5.cloned.1.call-done = bf16[256,576]{0,1:T(8,128)(2,1)} async-done(((bf16[2048,576]{0,1:T(8,128)(2,1)}), bf16[256,576]{0,1:T(8,128)(2,1)}) %reduce-scatter.5.cloned.1.call-update) | async-done | bytes 294928 | tf_op jit(solution)/shard_map/reduce_scatter | solution.py:48
  145.3 1.8 copy.59
  147.2 0.1 copy.56
  147.3 17.1 %reduce-scatter.7.cloned.1.call-done = bf16[128,576]{1,0:T(8,128)(2,1)} async-done(((bf16[256,576]{1,0:T(8,128)(2,1)}), bf16[128,576]{1,0:T(8,128)(2,1)}) %reduce-scatter.7.cloned.1.call-update) | async-done | bytes 147472
  164.4 1.1 copy.60
  165.5 0.7 reshape.163
  166.2 10.2 %all-to-all-start.3 = ((bf16[128,32,18]{0,2,1:T(8,128)(2,1)}), bf16[128,32,18]{0,2,1:T(8,128)(2,1)S(1)}, u32[]{:S(2)}, u32[]{:S(2)}) async-start(bf16[128,32,18]{0,2,1:T(8,128)(2,1)} %reshape.163), calls=%async_computation.4 | async-start | bytes 393216 | tf_op jit(solution)/shard_map/all_to_all | solution.py:151
  176.4 0.2 select_reduce_fusion
  176.6 0.1 reduce_sum.92
  176.7 0.7 copy.57
  177.4 11.1 %all-to-all-done.3 = bf16[128,32,18]{0,2,1:T(8,128)(2,1)S(1)} async-done(((bf16[128,32,18]{0,2,1:T(8,128)(2,1)}), bf16[128,32,18]{0,2,1:T(8,128)(2,1)S(1)}, u32[]{:S(2)}, u32[]{:S(2)}) %all-to-all-start.3) | async-done | bytes 147488 | tf_op jit(solution)/shard_map/all_to_all | solution.py:151
  188.6 0.1 reshape.164
  188.6 1.0 convolution_convert_fusion.2
  (51 shorter events, 0.5 us)
Async XLA Ops:
  7.2 78.5 %copy-start = (bf16[1,176,2048]{2,1,0:T(8,128)(2,1)S(1)}, bf16[1,176,2048]{2,1,0:T(8,128)(2,1)}, u32[]{:S(2)}) copy-start(bf16[1,176,2048]{2,1,0:T(8,128)(2,1)} %param.27) | copy-start | bytes 2162692
  7.2 1.5 copy-start.1
  7.2 1.7 copy-start.6
  7.2 74.7 %all-gather.2.cloned.1.call-start = ((), (), s32[]{:S(2)}) async-start(), calls=%async_computation.6 | async-start | bytes 2506752 | tf_op jit(solution)/shard_map/all_gather | solution.py:139
  42.7 102.7 %reduce-scatter.5.cloned.1.call-start = ((), (), s32[]{:S(2)}) async-start(), calls=%async_computation.7 | async-start | bytes 2654208 | tf_op jit(solution)/shard_map/reduce_scatter | solution.py:48
  81.9 3.8 %copy-start.8 = (bf16[576,2048]{1,0:T(8,128)(2,1)S(1)}, bf16[576,2048]{1,0:T(8,128)(2,1)}, u32[]{:S(2)}) copy-start(bf16[576,2048]{1,0:T(8,128)(2,1)} %all-gather.2.cloned.1.call-done) | copy-start | bytes 7077892
  90.4 1.0 copy-start.3
  90.4 1.2 copy-start.9
  90.4 1.2 copy-start.11
  90.4 1.8 copy-start.10
  91.5 4.5 %copy-start.5 = (f32[31,128]{1,0:T(8,128)S(1)}, f32[31,128]{1,0:T(8,128)}, u32[]{:S(2)}) copy-start(f32[31,128]{1,0:T(8,128)} %param.18) | copy-start | bytes 47620
  91.7 17.6 %copy-start.2 = (bf16[128,2048]{1,0:T(8,128)(2,1)S(1)}, bf16[128,2048]{1,0:T(8,128)(2,1)}, u32[]{:S(2)}) copy-start(bf16[128,2048]{1,0:T(8,128)(2,1)} %param.20) | copy-start | bytes 1572868
  91.7 17.6 %copy-start.7 = (f32[128]{0:T(128)S(1)}, f32[128]{0:T(128)}, u32[]{:S(2)}) copy-start(f32[128]{0:T(128)} %param.19) | copy-start | bytes 1540
  92.6 4.7 %collective-permute-start = (bf16[128,30]{0,1:T(8,128)(2,1)S(1)}, bf16[128,30]{0,1:T(8,128)(2,1)S(1)}, u32[]{:S(2)}, u32[]{:S(2)}) collective-permute-start(bf16[128,30]{0,1:T(8,128)(2,1)S(1)} %slice.270), channel_id=1, source_target_pairs={{0,16},{16,32},{32,48},{48,64},{64,80},{80,96},{96,112},{112,128},... | collective-permute-start | bytes 23048 | tf_op jit(solution)/shard_map/ppermute | solution.py:14
  97.6 49.7 %copy-start.4 = (f32[192,2]{0,1:T(2,128)S(1)}, f32[192,2]{0,1:T(2,128)}, u32[]{:S(2)}) copy-start(f32[192,2]{0,1:T(2,128)} %param.24) | copy-start | bytes 4612
  110.6 55.6 %all-to-all-start.1 = ((bf16[16,128,128]{1,2,0:T(8,128)(2,1)}), bf16[16,128,128]{1,2,0:T(8,128)(2,1)S(1)}, u32[]{:S(2)}, u32[]{:S(2)}) async-start(bf16[16,128,128]{1,2,0:T(8,128)(2,1)} %bitcast.112), calls=%async_computation.1 | async-start | bytes 1048576 | tf_op jit(solution)/shard_map/all_to_all | solution.py:41
  115.5 49.0 %reduce-scatter.7.cloned.1.call-start = ((), (), s32[]{:S(2)}) async-start(), calls=%async_computation.8 | async-start | bytes 491520
  166.2 22.3 %all-to-all-start.3 = ((bf16[128,32,18]{0,2,1:T(8,128)(2,1)}), bf16[128,32,18]{0,2,1:T(8,128)(2,1)S(1)}, u32[]{:S(2)}, u32[]{:S(2)}) async-start(bf16[128,32,18]{0,2,1:T(8,128)(2,1)} %reshape.163), calls=%async_computation.4 | async-start | bytes 393216 | tf_op jit(solution)/shard_map/all_to_all | solution.py:151
Sparse Core Ops, SparseCore 0:
  42.8 39.1 all-gather.1
  90.6 54.7 reduce-scatter.4
  148.1 16.2 reduce-scatter.6
where the time goes:
time: 197 us; the launch traced here: 196 us
  waiting for transfers between devices  98.6 us (50%)
  blocking collectives  36.2 us (18%)
  starting transfers between devices  18.5 us (9%)
  local copies, waits for them, and re-layouts  14.1 us (7%)
  between operations  14.1 us (7%)
  matrix products  10.6 us (5%)
  other arithmetic  3.98 us (2%)
    all_gather x1, waiting for transfers between devices, body(): arrived = lax.all_gather(arrived, TP, axis=1, tiled=True)  39.2 us
    reduce_scatter x1, waiting for transfers between devices, summed_rows(): so_far = lax.psum_scatter(so_far, axis, scatter_dimension=0, tiled=True)  29.8 us
    all_to_all x1, blocking collectives, body(): lax.all_to_all(send_rows, 'ep', split_axis=0, concat_axis=0, tiled=True)  24.6 us
    unnamed x4, waiting for transfers between devices  17.2 us
    all_to_all x1, blocking collectives, copy_for_each(): lax.all_to_all(jnp.broadcast_to(x[None], (peers, *x.shape)), axis, 0, 0,...  11.6 us
    all_to_all x1, waiting for transfers between devices, body(): lax.all_to_all(expert_rows.reshape(expert_rows.shape[0], experts, capacit...  11.1 us
    all_to_all x1, starting transfers between devices, body(): lax.all_to_all(expert_rows.reshape(expert_rows.shape[0], experts, capacit...  10.2 us
    all_to_all x1, starting transfers between devices, sum_at_owner(): tiles = lax.all_to_all(in_blocks(x, dim, peers), axis, 0, 0, tiled=True)  4.82 us
  transfers between devices with their start and end apart: 6, of which 5 were waited for; matrix products, arithmetic and copies ran while one was open for 4% of the time, Pallas kernels for 0%

commit v1 on v0

--- a/solution.py
+++ b/solution.py
@@ -136,7 +136,9 @@
     arrived = lax.all_to_all(send_rows, "ep", split_axis=0, concat_axis=0, tiled=True).reshape(
         experts * capacity, -1
     )
-    arrived = lax.all_gather(arrived, TP, axis=1, tiled=True)
+    arrived = jnp.concatenate(
+        lax.all_to_all(jnp.stack([arrived] * lax.axis_size(TP)), TP, 0, 0), axis=1
+    )
     gate_act = jnp.dot(arrived, gate_local, preferred_element_type=jnp.float32)
     up_act = jnp.dot(arrived, up_local, preferred_element_type=jnp.float32)
     hidden = (jax.nn.silu(gate_act) * up_act).astype(jnp.bfloat16)

time: 197 us -> 211 us (1.071)
  blocking collectives: 36.2 us -> 97.9 us
  waiting for transfers between devices: 98.6 us -> 54.3 us
    all_to_all x0 -> x1, blocking collectives: none -> 62.2 us  [body(): lax.all_to_all(jnp.stack([arrived] * lax.axis_size(TP)), TP, 0, 0)]
    all_gather x1 -> x0, waiting for transfers between devices: 39.2 us -> none  [body(): arrived = lax.all_gather(arrived, TP, axis=1, tiled=True)]
    reduce_scatter x1, waiting for transfers between devices: 29.8 us -> 24.3 us  [summed_rows(): so_far = lax.psum_scatter(so_far, axis, scatter_dimension=0, tiled=True)]
    unnamed x4 -> x3, waiting for transfers between devices: 17.2 us -> 17.5 us
  transfers between devices with their start and end apart: 6 -> 5, of which waited for: 5 -> 4; matrix products, arithmetic and copies ran while one was open for 4% -> 4% of each run, Pallas kernels for 0% -> 0%
where the time goes in v1:
time: 211 us; the launch traced here: 210 us
  blocking collectives  97.9 us (46%)
  waiting for transfers between devices  54.3 us (26%)
  starting transfers between devices  17 us (8%)
  between operations  14.4 us (7%)
  local copies, waits for them, and re-layouts  13.9 us (7%)
  matrix products  8.58 us (4%)
  other arithmetic  3.98 us (2%)
    all_to_all x1, blocking collectives, body(): lax.all_to_all(jnp.stack([arrived] * lax.axis_size(TP)), TP, 0, 0)  62.2 us
    all_to_all x1, blocking collectives, body(): lax.all_to_all(send_rows, 'ep', split_axis=0, concat_axis=0, tiled=True)  24.6 us
    reduce_scatter x1, waiting for transfers between devices, summed_rows(): so_far = lax.psum_scatter(so_far, axis, scatter_dimension=0, tiled=True)  24.3 us
    unnamed x3, waiting for transfers between devices  17.5 us
    all_to_all x1, waiting for transfers between devices, body(): lax.all_to_all(expert_rows.reshape(expert_rows.shape[0], experts, capacit...  11.1 us
    all_to_all x1, blocking collectives, copy_for_each(): lax.all_to_all(jnp.broadcast_to(x[None], (peers, *x.shape)), axis, 0, 0,...  11.1 us
    all_to_all x1, starting transfers between devices, body(): lax.all_to_all(expert_rows.reshape(expert_rows.shape[0], experts, capacit...  10.2 us
    all_to_all x1, starting transfers between devices, sum_at_owner(): tiles = lax.all_to_all(in_blocks(x, dim, peers), axis, 0, 0, tiled=True)  4.87 us
  transfers between devices with their start and end apart: 5, of which 4 were waited for; matrix products, arithmetic and copies ran while one was open for 4% of the time, Pallas kernels for 0%

profile of v1, /device:TPU:8, one launch (start us, length us, event | category | flops | bytes accessed | tf_op | source)
XLA Modules:
  0.0 210.1 jit_solution(12220497322713236495)
XLA Ops:
  7.2 1.4 convert_element_type.61
  8.7 0.2 multiply_reduce_fusion
  8.9 0.1 copy.54
  9.0 0.1 eq.43
  9.2 0.1 eq.39
  9.3 0.9 reduce-window.6
  10.2 0.2 slice_reduce_fusion
  10.5 0.1 fusion.70
  10.6 0.1 reduce_sum.96
  10.8 0.1 mul.528
  10.9 2.9 %scatter_custom_fusion = s32[576]{0:T(1024)S(1)} fusion(s32[384]{0:T(512)S(1)} %fusion.82, s32[384]{0:T(512)S(1)} %fusion.76, s32[]{:T(128)} %constant.74.clone.1), kind=kCustom, calls=%fused_computation.135 | custom fusion | bytes 2308 | tf_op jit(solution)/shard_map/scatter | solution.py:119
  13.9 0.8 dynamic-slice
  14.7 0.1 fusion.37
  14.8 1.9 gather_fusion
  16.8 0.1 broadcast_in_dim.29
  16.9 0.1 broadcast_in_dim.50
  17.0 0.3 select_select_fusion
  17.3 24.6 %all_to_all.26 = bf16[32,18,128]{2,1,0:T(8,128)(2,1)S(1)} all-to-all(bf16[32,18,128]{2,1,0:T(8,128)(2,1)S(1)} %select_select_fusion), channel_id=1, replica_groups=mesh['ep'=32,'tp_0'=8,'tp_1'=2] {'ep'}, dimensions={0} | all-to-all | bytes 294912 | tf_op jit(solution)/shard_map/all_to_all | solution.py:136
  41.9 0.1 stack_reshape.2
  42.0 0.4 stack.3
  42.4 62.2 %all_to_all.27 = bf16[16,576,128]{2,1,0:T(8,128)(2,1)S(1)} all-to-all(bf16[16,576,128]{2,1,0:T(8,128)(2,1)S(1)} %stack.3), channel_id=1, replica_groups=mesh['ep'=32,'tp_0'=8,'tp_1'=2] {'tp_0','tp_1'}, dimensions={0} | all-to-all | bytes 4718592 | tf_op jit(solution)/shard_map/all_to_all | solution.py:140
  104.6 1.8 fusion.3
  106.4 4.7 %fusion = bf16[2048,576]{0,1:T(8,128)(2,1)} fusion(bf16[1,176,2048]{2,1,0:T(8,128)(2,1)S(1)} %copy-done, bf16[1,2048,176]{1,2,0:T(8,128)(2,1)} %param.26, f32[576,176]{0,1:T(8,128)} %fusion.3, bf16[16,576,128]{2,1,0:T(8,128)(2,1)S(1)} %all_to_all.27), kind=kOutput, calls=%fused_computation.3 | convolution fusion | flops 832260096 | bytes 6565888 | tf_op jit(solution)/shard_map/dot_general | solution.py:148
  111.2 1.0 copy-done.3
  112.2 0.2 fusion.21
  112.4 0.4 fusion.18
  112.8 0.1 copy.50
  112.9 0.4 fusion.20
  113.3 1.9 collective-permute-start
  115.2 1.3 collective-permute-done
  116.6 0.3 fusion.88
  116.9 11.1 %all_to_all.28 = f32[16,1,256]{2,1,0:T(1,128)S(1)} all-to-all(f32[16,1,256]{2,1,0:T(1,128)S(1)} %broadcast_in_dim.28), channel_id=1, replica_groups=mesh['ep'=32,'tp_0'=8,'tp_1'=2] {'tp_0','tp_1'}, dimensions={0} | all-to-all | bytes 32768 | tf_op jit(solution)/shard_map/all_to_all | solution.py:19
  128.0 0.4 fusion.7
  128.4 0.9 copy.87
  129.3 4.9 %all-to-all-start.1 = ((bf16[16,128,128]{1,2,0:T(8,128)(2,1)}), bf16[16,128,128]{1,2,0:T(8,128)(2,1)S(1)}, u32[]{:S(2)}, u32[]{:S(2)}) async-start(bf16[16,128,128]{1,2,0:T(8,128)(2,1)} %bitcast.130), calls=%async_computation.1 | async-start | bytes 1048576 | tf_op jit(solution)/shard_map/all_to_all | solution.py:41
  134.3 24.3 %reduce-scatter.5.cloned.1.call-done = bf16[256,576]{0,1:T(8,128)(2,1)} async-done(((bf16[2048,576]{0,1:T(8,128)(2,1)}), bf16[256,576]{0,1:T(8,128)(2,1)}) %reduce-scatter.5.cloned.1.call-update) | async-done | bytes 294928 | tf_op jit(solution)/shard_map/reduce_scatter | solution.py:48
  158.6 1.8 copy.62
  160.5 0.1 copy.59
  160.6 17.5 %reduce-scatter.7.cloned.1.call-done = bf16[128,576]{1,0:T(8,128)(2,1)} async-done(((bf16[256,576]{1,0:T(8,128)(2,1)}), bf16[128,576]{1,0:T(8,128)(2,1)}) %reduce-scatter.7.cloned.1.call-update) | async-done | bytes 147472
  178.1 1.1 copy.63
  179.1 0.7 reshape.169
  179.9 10.2 %all-to-all-start.4 = ((bf16[128,32,18]{0,2,1:T(8,128)(2,1)}), bf16[128,32,18]{0,2,1:T(8,128)(2,1)S(1)}, u32[]{:S(2)}, u32[]{:S(2)}) async-start(bf16[128,32,18]{0,2,1:T(8,128)(2,1)} %reshape.169), calls=%async_computation.5 | async-start | bytes 393216 | tf_op jit(solution)/shard_map/all_to_all | solution.py:153
  190.1 0.2 select_reduce_fusion
  190.3 0.1 reduce_sum.92
  190.4 0.7 copy.60
  191.1 11.1 %all-to-all-done.4 = bf16[128,32,18]{0,2,1:T(8,128)(2,1)S(1)} async-done(((bf16[128,32,18]{0,2,1:T(8,128)(2,1)}), bf16[128,32,18]{0,2,1:T(8,128)(2,1)S(1)}, u32[]{:S(2)}, u32[]{:S(2)}) %all-to-all-start.4) | async-done | bytes 147488 | tf_op jit(solution)/shard_map/all_to_all | solution.py:153
  202.2 0.1 reshape.170
  202.3 1.0 convolution_convert_fusion.2
  (50 shorter events, 0.5 us)
Async XLA Ops:
  7.2 99.2 %copy-start = (bf16[1,176,2048]{2,1,0:T(8,128)(2,1)S(1)}, bf16[1,176,2048]{2,1,0:T(8,128)(2,1)}, u32[]{:S(2)}) copy-start(bf16[1,176,2048]{2,1,0:T(8,128)(2,1)} %param.27) | copy-start | bytes 2162692
  7.2 1.5 copy-start.1
  7.2 1.7 copy-start.6
  7.2 151.4 %reduce-scatter.5.cloned.1.call-start = ((), (), s32[]{:S(2)}) async-start(), calls=%async_computation.7 | async-start | bytes 2654208 | tf_op jit(solution)/shard_map/reduce_scatter | solution.py:48
  42.4 62.2 %copy-start.8 = (bf16[1,2048,176]{1,2,0:T(8,128)(2,1)S(1)}, bf16[1,2048,176]{1,2,0:T(8,128)(2,1)}, u32[]{:S(2)}) copy-start(bf16[1,2048,176]{1,2,0:T(8,128)(2,1)} %param.25) | copy-start | bytes 2162692
  111.1 1.0 copy-start.3
  111.1 1.2 copy-start.9
  111.1 1.2 copy-start.11
  111.1 1.8 copy-start.10
  112.2 3.0 %copy-start.5 = (f32[31,128]{1,0:T(8,128)S(1)}, f32[31,128]{1,0:T(8,128)}, u32[]{:S(2)}) copy-start(f32[31,128]{1,0:T(8,128)} %param.18) | copy-start | bytes 47620
  112.4 15.6 %copy-start.2 = (bf16[128,2048]{1,0:T(8,128)(2,1)S(1)}, bf16[128,2048]{1,0:T(8,128)(2,1)}, u32[]{:S(2)}) copy-start(bf16[128,2048]{1,0:T(8,128)(2,1)} %param.20) | copy-start | bytes 1572868
  112.4 15.6 %copy-start.7 = (f32[128]{0:T(128)S(1)}, f32[128]{0:T(128)}, u32[]{:S(2)}) copy-start(f32[128]{0:T(128)} %param.19) | copy-start | bytes 1540
  113.3 3.2 %collective-permute-start = (bf16[128,30]{0,1:T(8,128)(2,1)S(1)}, bf16[128,30]{0,1:T(8,128)(2,1)S(1)}, u32[]{:S(2)}, u32[]{:S(2)}) collective-permute-start(bf16[128,30]{0,1:T(8,128)(2,1)S(1)} %slice.270), channel_id=1, source_target_pairs={{0,16},{16,32},{32,48},{48,64},{64,80},{80,96},{96,112},{112,128},... | collective-permute-start | bytes 23048 | tf_op jit(solution)/shard_map/ppermute | solution.py:14
  116.8 43.7 %copy-start.4 = (f32[192,2]{0,1:T(2,128)S(1)}, f32[192,2]{0,1:T(2,128)}, u32[]{:S(2)}) copy-start(f32[192,2]{0,1:T(2,128)} %param.24) | copy-start | bytes 4612
  129.3 50.5 %all-to-all-start.1 = ((bf16[16,128,128]{1,2,0:T(8,128)(2,1)}), bf16[16,128,128]{1,2,0:T(8,128)(2,1)S(1)}, u32[]{:S(2)}, u32[]{:S(2)}) async-start(bf16[16,128,128]{1,2,0:T(8,128)(2,1)} %bitcast.130), calls=%async_computation.1 | async-start | bytes 1048576 | tf_op jit(solution)/shard_map/all_to_all | solution.py:41
  134.2 43.9 %reduce-scatter.7.cloned.1.call-start = ((), (), s32[]{:S(2)}) async-start(), calls=%async_computation.8 | async-start | bytes 491520
  179.9 22.4 %all-to-all-start.4 = ((bf16[128,32,18]{0,2,1:T(8,128)(2,1)}), bf16[128,32,18]{0,2,1:T(8,128)(2,1)S(1)}, u32[]{:S(2)}, u32[]{:S(2)}) async-start(bf16[128,32,18]{0,2,1:T(8,128)(2,1)} %reshape.169), calls=%async_computation.5 | async-start | bytes 393216 | tf_op jit(solution)/shard_map/all_to_all | solution.py:153
Sparse Core Ops, SparseCore 0:
  111.3 47.2 reduce-scatter.4
  161.4 16.6 reduce-scatter.6
